TPU v7x, 32 devices: a whole 2x2x4 slice. The times are simulated.
32 devices in a mesh: sp: 8 (over z, x), tp: 4 (over y, core).
Axes of the slice: x: 2, y: 2, z: 4, core: 2. Of those that a mesh axis runs over, the one named last changes fastest.
Arguments:
- queries: bfloat16 [4096, 512], P('sp', 'tp'), may hold values from -9.5625 to 9.5625
- keys: bfloat16 [4096, 512], P('sp', 'tp'), may hold values from -9.5625 to 9.5625
- values: bfloat16 [4096, 512], P('sp', 'tp'), may hold values from -6 to 6
- key_bias: bfloat16 [4096, 8], P('sp', 'tp'), may hold values from -17 to 0
- residual: bfloat16 [4096, 2048], P(('sp', 'tp')), may hold values from -6 to 6
- out_weight: bfloat16 [512, 2048], replicated, may hold values from -1 to 1
- norm_gain: float32 [2048], replicated, may hold values from 0.1 to 1.9
- routes: int32 [4096, 2], P(('sp', 'tp')), may hold values from 0 to 7, all different within a row; in each aligned block of 128 rows (0 to 127, 128 to 255, ...) at most 40 rows name the same one
- route_weights: float32 [4096, 2], P(('sp', 'tp')), may hold values from 0.25 to 2
- gate_weight: bfloat16 [8, 2048, 4096], P('sp', None, 'tp'), may hold values from -0.125 to 0.125
- up_weight: bfloat16 [8, 2048, 4096], P('sp', None, 'tp'), may hold values from -0.125 to 0.125
- down_weight: bfloat16 [8, 4096, 2048], P('sp', 'tp'), may hold values from -0.09375 to 0.09375
Outputs:
- output: bfloat16 [4096, 2048], P(('sp', 'tp'))
Inputs may be any that keep to these rules, and one draw needn't show every extreme that they name: `routes`: each row names 2 different experts; the rows of one device name no expert more than 40 times.
All inputs are finite; a program needn't handle non-finite values.
Results may differ from a plain program's by a relative error of at most 0.017.
Values may be sent and summed in bfloat16 or wider, within the bound.
A program may use at most 128 MiB of HBM per device.

v0:
```python
import jax
import jax.numpy as jnp
from jax import lax
from jax.sharding import PartitionSpec as P

HEAD_DIM = 64
TOP = 2
SPAN = 512


epsilon = 1e-06


def shards(
    queries,
    keys,
    values,
    key_bias,
    residual,
    out_weight,
    norm_gain,
    routes,
    route_weights,
    gate_weight,
    up_weight,
    down_weight,
):
    shard_len = queries.shape[0]
    local_heads = key_bias.shape[1]
    sp_count = lax.axis_size("sp")
    offset = lax.axis_index("sp") * shard_len
    query_heads = queries.reshape(shard_len, local_heads, HEAD_DIM)
    query_pos = offset + lax.iota(jnp.int32, shard_len)
    score_scale = HEAD_DIM ** (-0.5)
    slot_count = sp_count * shard_len // SPAN

    def span_terms(key_rows, value_rows, bias_rows, key_first):
        scores = jnp.einsum(
            "qhd,khd->qhk",
            query_heads,
            key_rows.reshape(SPAN, local_heads, HEAD_DIM),
            preferred_element_type=jnp.float32,
        )
        scores = scores * score_scale + jnp.transpose(bias_rows.astype(jnp.float32))[None, :, :]
        key_pos = key_first + lax.iota(jnp.int32, SPAN)
        earlier = key_pos[None, None, :] < query_pos[:, None, None]
        failure = jnp.where(earlier, jax.nn.log_sigmoid(-scores), 0.0)
        later_sum = lax.cumsum(failure, axis=2, reverse=True) - failure
        weights = jnp.where(earlier, jnp.exp(jax.nn.log_sigmoid(scores) + later_sum), 0.0).astype(
            jnp.bfloat16
        )
        span_out = jnp.einsum(
            "qhk,khd->qhd",
            weights,
            value_rows.reshape(SPAN, local_heads, HEAD_DIM),
            preferred_element_type=jnp.float32,
        )
        return (span_out, jnp.sum(failure, axis=2))

    def skipped():
        return (
            jnp.zeros((shard_len, local_heads, HEAD_DIM), jnp.float32),
            jnp.zeros((shard_len, local_heads), jnp.float32),
        )

    empty_pair = (
        jnp.zeros((slot_count, shard_len, local_heads, HEAD_DIM), jnp.float32),
        jnp.zeros((slot_count, shard_len, local_heads), jnp.float32),
    )
    key_piece = lax.all_gather(keys, "sp", axis=0, tiled=True)
    value_piece = lax.all_gather(values, "sp", axis=0, tiled=True)
    bias_piece = lax.all_gather(key_bias, "sp", axis=0, tiled=True)
    span_total = key_piece.shape[0] // SPAN

    def place_span(which, held):
        outs_held, totals_held = held
        row_begin = which * SPAN

        def compute():
            return span_terms(
                lax.dynamic_slice_in_dim(key_piece, row_begin, SPAN, 0),
                lax.dynamic_slice_in_dim(value_piece, row_begin, SPAN, 0),
                lax.dynamic_slice_in_dim(bias_piece, row_begin, SPAN, 0),
                row_begin,
            )

        span_out, span_sum = lax.cond(row_begin < offset + shard_len, compute, skipped)
        slot = row_begin // SPAN
        return (
            lax.dynamic_update_index_in_dim(outs_held, span_out, slot, 0),
            lax.dynamic_update_index_in_dim(totals_held, span_sum, slot, 0),
        )

    span_outs, span_sums = lax.fori_loop(0, span_total, place_span, empty_pair)
    after_span = lax.cumsum(span_sums, axis=0, reverse=True) - span_sums
    attended = jnp.sum(jnp.exp(after_span)[..., None] * span_outs, axis=0)
    attended = attended.reshape(shard_len, local_heads * HEAD_DIM).astype(jnp.bfloat16)
    token_heads = lax.all_to_all(attended, "tp", split_axis=0, concat_axis=1, tiled=True)
    projected = jnp.dot(token_heads, out_weight, preferred_element_type=jnp.float32)
    stream = (residual.astype(jnp.float32) + projected).astype(jnp.bfloat16).astype(jnp.float32)
    normed = (
        stream * lax.rsqrt(jnp.mean(stream * stream, axis=-1, keepdims=True) + epsilon) * norm_gain
    ).astype(jnp.bfloat16)
    token_count = residual.shape[0]
    width_model = residual.shape[1]
    capacity = max(2, 5 * token_count * TOP // (4 * sp_count))
    flat_routes = routes.reshape(-1)
    onehot = (flat_routes[:, None] == lax.iota(jnp.int32, sp_count)[None, :]).astype(jnp.int32)
    before = jnp.cumsum(onehot, axis=0) - onehot
    slot_of = flat_routes * capacity + jnp.sum(before * onehot, axis=1)
    select = (slot_of[:, None] == lax.iota(jnp.int32, sp_count * capacity)[None, :]).astype(
        jnp.bfloat16
    )
    placing = jnp.sum(select.reshape(token_count, TOP, sp_count * capacity), axis=1)
    outgoing = jnp.einsum("ts,td->sd", placing, normed, preferred_element_type=jnp.float32).astype(
        jnp.bfloat16
    )
    arrived = lax.all_to_all(outgoing, "sp", split_axis=0, concat_axis=0, tiled=True)
    row_block = lax.all_gather(arrived, "tp", axis=0, tiled=True)
    gate_act = jnp.dot(row_block, gate_weight[0], preferred_element_type=jnp.float32)
    up_act = jnp.dot(row_block, up_weight[0], preferred_element_type=jnp.float32)
    hidden = (jax.nn.silu(gate_act) * up_act).astype(jnp.bfloat16)
    partial_value = jnp.dot(hidden, down_weight[0], preferred_element_type=jnp.float32)
    summed = lax.psum_scatter(
        lax.optimization_barrier(partial_value.astype(jnp.bfloat16))
        .astype(jnp.float32)
        .astype(jnp.bfloat16),
        "tp",
        scatter_dimension=0,
        tiled=True,
    )
    returned = lax.all_to_all(summed, "sp", split_axis=0, concat_axis=0, tiled=True)
    picked = jnp.dot(select, returned, preferred_element_type=jnp.float32).reshape(
        token_count, TOP, width_model
    )
    routed = jnp.sum(picked * route_weights[:, :, None], axis=1)
    return (stream + routed).astype(jnp.bfloat16)


def solution(mesh):
    return jax.shard_map(
        shards,
        mesh=mesh,
        in_specs=(
            P("sp", "tp"),
            P("sp", "tp"),
            P("sp", "tp"),
            P("sp", "tp"),
            P(("sp", "tp"), None),
            P(),
            P(),
            P(("sp", "tp"), None),
            P(("sp", "tp"), None),
            P("sp", None, "tp"),
            P("sp", None, "tp"),
            P("sp", "tp", None),
        ),
        out_specs=P(("sp", "tp"), None),
        check_vma=False,
    )
```

profile of v0, /device:TPU:0, one launch (start us, length us, event | category | flops | bytes accessed | tf_op | source)
XLA Modules:
  0.0 488.3 jit_solution(3065898955620560094)
XLA Ops:
  6.5 1.8 copy.63
  8.4 1.7 copy.62
  10.1 0.8 copy.66
  12.3 1.0 copy.64
  13.4 28.3 %all_gather.14 = bf16[4096,2]{0,1:T(2,128)(2,1)S(1)} all-gather(bf16[512,2]{0,1:T(2,128)(2,1)} %param.19), channel_id=1, replica_groups=mesh['sp'=8,'tp'=4] {'sp'}, dimensions={0}, use_global_device_ids=true | all-gather | bytes 18432 | tf_op jit(solution)/shard_map/all_gather | solution.py:72
  42.3 9.2 %all-gather.6.cloned.1.call-done = bf16[4096,128]{0,1:T(8,128)(2,1)} async-done(((bf16[512,128]{0,1:T(8,128)(2,1)}), bf16[4096,128]{0,1:T(8,128)(2,1)}) %all-gather.6.cloned.1.call-update) | async-done | bytes 1048592 | tf_op jit(solution)/shard_map/all_gather | solution.py:70
  51.6 40.3 %all-gather.4.cloned.1.call-done = bf16[4096,128]{0,1:T(8,128)(2,1)} async-done(((bf16[512,128]{0,1:T(8,128)(2,1)}), bf16[4096,128]{0,1:T(8,128)(2,1)}) %all-gather.4.cloned.1.call-update) | async-done | bytes 1048592 | tf_op jit(solution)/shard_map/all_gather | solution.py:71
  91.9 1.6 broadcast_in_dim.56
  93.5 28.5 %while.18 = (s32[]{:T(128)}, f32[8,512,2,64]{1,3,2,0:T(8,128)}, f32[8,512,2]{1,2,0:T(2,128)S(1)}, s32[]{:T(128)}, bf16[4096,128]{0,1:T(8,128)(2,1)}, /*index=5*/...) while((s32[]{:T(128)}, f32[8,512,2,64]{1,3,2,0:T(8,128)}, ...), condition=%wide.region_6.7_spmd.clone, body=%wide.region_0.6_spmd.clone.sunk | while | flops 218906624 | bytes 42494496 | solution.py:94
  93.5 22.3 %conditional.3 = (f32[1,512,2,64]{1,3,2,0:T(8,128)S(1)}, f32[1,512,2]{1,2,0:T(2,128)S(1)}) conditional(s32[]{:T(128)} %convert_element_type.94, () %tuple.60, (s32[]{:T(128)}, bf16[4096,128]{0,1:T(8,128)(2,1)}, s32[]{:T(128)}, bf16[4096,128]{0,1:T(8,128)(2,1)}, bf16[512,2,64]{0,2,1:T(8,128)(2,1)S(1)}, /*index=5*/bf16[4096,2]{0,1:T(2,128)(2,1)S(1)}, ...), branch_computations={%region_1.0_spmd, %region_2.5_spmd} | conditional | flops 218906624 | bytes 41959552 | solution.py:87
  93.5 1.0 constant_dynamic-slice_fusion
  94.7 3.0 fusion.15
  97.8 9.6 %fusion.13 = f32[512,2,4,128]{0,2,1,3:T(4,128)S(1)} fusion(f32[512,2,4,128]{0,3,2,1:T(8,128)S(1)} %bitcast.89), kind=kOutput, calls=%fused_computation.18 | output fusion | flops 66584576 | bytes 4194304 | tf_op jit(solution)/shard_map/reduce-window
  107.4 1.3 copy-done.1
  108.8 1.8 broadcast_add_fusion
  110.6 1.2 copy.60
  112.2 3.2 fusion.6
  118.1 0.7 constant_dynamic-update-slice_fusion.4
  118.9 0.7 constant_dynamic-update-slice_fusion.4
  119.7 0.7 constant_dynamic-update-slice_fusion.4
  122.0 1.8 multiply_reduce_fusion
  124.6 3.5 all-to-all-start
  128.2 4.5 all-to-all-done
  132.6 1.6 multiply_reduce_fusion.1
  134.8 190.0 %all_to_all.40 = bf16[8,40,2048]{2,1,0:T(8,128)(2,1)} all-to-all(bf16[8,40,2048]{2,1,0:T(8,128)(2,1)S(1)} %bitcast.92), channel_id=1, replica_groups=mesh['sp'=8,'tp'=4] {'sp'}, dimensions={0} | all-to-all | bytes 2621440 | tf_op jit(solution)/shard_map/all_to_all | solution.py:118
  324.9 38.8 %all-gather.8.cloned.1.call-done = bf16[1280,2048]{1,0:T(8,128)(2,1)} async-done(((bf16[320,2048]{1,0:T(8,128)(2,1)}), bf16[1280,2048]{1,0:T(8,128)(2,1)}) %all-gather.8.cloned.1.call-update) | async-done | bytes 5242896 | tf_op jit(solution)/shard_map/all_gather | solution.py:119
  363.7 10.2 %fusion.18 = f32[1280,1024]{1,0:T(8,128)} fusion(bf16[1280,2048]{1,0:T(8,128)(2,1)} %all-gather.8.cloned.1.call-done, bf16[1,2048,1024]{2,1,0:T(8,128)(2,1)} %param.25), kind=kOutput, calls=%fused_computation.37 | convolution fusion | flops 5368709120 | bytes 14680064 | tf_op jit(solution)/shard_map/dot_general | solution.py:120
  373.9 18.0 %convolution_convert_fusion = bf16[1280,2048]{1,0:T(8,128)(2,1)} fusion(bf16[1,1024,2048]{2,1,0:T(8,128)(2,1)} %param.27, f32[1280,1024]{1,0:T(8,128)} %fusion.18, bf16[1280,2048]{1,0:T(8,128)(2,1)} %all-gather.8.cloned.1.call-done, bf16[1,2048,1024]{2,1,0:T(8,128)(2,1)} %param.26), kind=kOutput, calls=%fused_computation.33 | convolution fusion | flops 10747904000 | bytes 24117248 | tf_op jit(solution)/shard_map/dot_general | solution.py:123
  391.9 51.5 %reduce-scatter.2.cloned.1.call-done = bf16[320,2048]{1,0:T(8,128)(2,1)} async-done(((bf16[1280,2048]{1,0:T(8,128)(2,1)}), bf16[320,2048]{1,0:T(8,128)(2,1)}) %reduce-scatter.2.cloned.1.call-update) | async-done | bytes 1310736 | tf_op jit(solution)/shard_map/reduce_scatter | solution.py:124
  443.4 36.7 %all_to_all.41 = bf16[8,40,2048]{2,1,0:T(8,128)(2,1)S(1)} all-to-all(bf16[8,40,2048]{2,1,0:T(8,128)(2,1)} %bitcast.95), channel_id=1, replica_groups=mesh['sp'=8,'tp'=4] {'sp'}, dimensions={0} | all-to-all | bytes 2621440 | tf_op jit(solution)/shard_map/all_to_all | solution.py:132
  480.1 0.8 fusion.24
  480.9 0.9 add_convert_fusion
  (84 shorter events, 8.7 us)
Async XLA Ops:
  6.5 126.1 %copy-start = (bf16[512,2048]{1,0:T(8,128)(2,1)S(1)}, bf16[512,2048]{1,0:T(8,128)(2,1)}, u32[]{:S(2)}) copy-start(bf16[512,2048]{1,0:T(8,128)(2,1)} %param.21) | copy-start | bytes 6291460
  6.5 45.0 %all-gather.6.cloned.1.call-start = ((), (), s32[]{:S(2)}) async-start(), calls=%async_computation.5 | async-start | bytes 1179648 | tf_op jit(solution)/shard_map/all_gather | solution.py:70
  8.4 83.5 %all-gather.4.cloned.1.call-start = ((), (), s32[]{:S(2)}) async-start(), calls=%async_computation.4 | async-start | bytes 1179648 | tf_op jit(solution)/shard_map/all_gather | solution.py:71
  107.4 1.3 copy-start.1
  110.6 1.6 copy-start.2
  124.6 9.6 %copy-start.3 = (f32[2048]{0:T(1024)S(1)}, f32[2048]{0:T(1024)}, u32[]{:S(2)}) copy-start(f32[2048]{0:T(1024)} %param.22) | copy-start | bytes 24580
  124.6 8.0 %all-to-all-start = ((bf16[4,128,128]{1,2,0:T(8,128)(2,1)}), bf16[4,128,128]{1,2,0:T(8,128)(2,1)S(1)}, u32[]{:S(2)}, u32[]{:S(2)}) async-start(bf16[4,128,128]{1,2,0:T(8,128)(2,1)} %copy.65), calls=%async_computation | async-start | bytes 262144 | tf_op jit(solution)/shard_map/all_to_all | solution.py:98
  128.1 235.7 %all-gather.8.cloned.1.call-start = ((), (), s32[]{:S(2)}) async-start(), calls=%async_computation.6 | async-start | bytes 6553600 | tf_op jit(solution)/shard_map/all_gather | solution.py:119
  324.8 118.6 %reduce-scatter.2.cloned.1.call-start = ((), (), s32[]{:S(2)}) async-start(), calls=%async_computation.7 | async-start | bytes 6553600 | tf_op jit(solution)/shard_map/reduce_scatter | solution.py:124
  391.9 88.2 %copy-start.4 = (f32[128,2]{0,1:T(2,128)S(1)}, f32[128,2]{0,1:T(2,128)}, u32[]{:S(2)}) copy-start(f32[128,2]{0,1:T(2,128)} %param.24) | copy-start | bytes 3076
Sparse Core Ops, SparseCore 0:
  9.4 42.1 all-gather.5
  53.6 38.1 all-gather.3
  325.0 38.7 all-gather.7
  392.0 51.3 reduce-scatter.1
where the time goes:
time: 489 us; the launch traced here: 488 us
  blocking collectives  255 us (52%)
  waiting for transfers between devices  144 us (29%)
  matrix products  34.4 us (7%)
  other arithmetic  19.2 us (4%)
  local copies, waits for them, and re-layouts  18.3 us (4%)
  between operations  13.2 us (3%)
    all_to_all x1, blocking collectives, shards(): lax.all_to_all(outgoing, 'sp', split_axis=0, concat_axis=0, tiled=True)  190 us
    reduce_scatter x1, waiting for transfers between devices, shards(): lax.psum_scatter(lax.optimization_barrier(partial_value.astype(jnp.bfloat...  51.5 us
    all_gather x1, waiting for transfers between devices, shards(): value_piece = lax.all_gather(values, 'sp', axis=0, tiled=True)  40.3 us
    all_gather x1, waiting for transfers between devices, shards(): row_block = lax.all_gather(arrived, 'tp', axis=0, tiled=True)  38.8 us
    all_to_all x1, blocking collectives, shards(): lax.all_to_all(summed, 'sp', split_axis=0, concat_axis=0, tiled=True)  36.7 us
    all_gather x1, blocking collectives, shards(): bias_piece = lax.all_gather(key_bias, 'sp', axis=0, tiled=True)  28.3 us
    dot_general x1, matrix products, shards(): jnp.dot(hidden, down_weight[0], preferred_element_type=jnp.float32)  18 us
    another operation x4, other arithmetic  10.3 us
  transfers between devices with their start and end apart: 5, of which 5 were waited for; matrix products, arithmetic and copies ran while one was open for 1% of the time, Pallas kernels for 0%

commit v1 on v0

v1 whole, which is shorter than its diff:
```python
import functools

import jax
import jax.numpy as jnp
from jax import lax
from jax.experimental import pallas as pl
from jax.experimental.pallas import tpu as pltpu
from jax.sharding import PartitionSpec as P

HEAD_DIM = 64
TOP = 2
SPAN = 512
BLOCK = 256
QUERY_ROWS = 256
BIAS_ROWS = 16
MESH = pl.DeviceIdType.MESH


epsilon = 1e-06


def attend_kernel(
    n, length, heads, q_ref, own_ref, out_ref, held, total, after, tri, up_sem, side_sem, recv_sem
):
    me = lax.axis_index("sp")
    odd = lax.rem(me, 2)
    partner = me + 1 - 2 * odd
    has_up = me + 2 < n
    has_down = me >= 2
    barrier = pltpu.get_barrier_semaphore()

    def greet(device):
        pl.semaphore_signal(barrier, inc=1, device_id={"sp": device}, device_id_type=MESH)

    greet(partner)
    pl.when(has_up)(lambda: greet(me + 2))
    pl.when(has_down)(lambda: greet(me - 2))

    total[...] = jnp.zeros_like(total)
    after[...] = jnp.zeros_like(after)
    tri_row = lax.broadcasted_iota(jnp.int32, (BLOCK, BLOCK), 0)
    tri_col = lax.broadcasted_iota(jnp.int32, (BLOCK, BLOCK), 1)
    tri[...] = (tri_row > tri_col).astype(jnp.float32).astype(jnp.bfloat16)

    pl.semaphore_wait(barrier, 1 + has_up.astype(jnp.int32) + has_down.astype(jnp.int32))

    def up(d, source):
        return pltpu.make_async_remote_copy(
            src_ref=source,
            dst_ref=held.at[d + 2],
            send_sem=up_sem.at[d],
            recv_sem=recv_sem.at[d + 2],
            device_id={"sp": me + 2},
            device_id_type=MESH,
        )

    def side(d, slot, source):
        return pltpu.make_async_remote_copy(
            src_ref=source,
            dst_ref=held.at[slot],
            send_sem=side_sem.at[d],
            recv_sem=recv_sem.at[slot],
            device_id={"sp": partner},
            device_id_type=MESH,
        )

    def send(d, source):
        pl.when(has_up)(lambda: up(d, source).start())
        pl.when(odd == 0)(lambda: side(d, d + 1, source).start())
        pl.when((odd == 1) & (d >= 2))(lambda: side(d, d - 1, source).start())

    width = heads * HEAD_DIM
    row_width = 2 * width
    lane = lax.broadcasted_iota(jnp.int32, (QUERY_ROWS, width), 1)
    tile_blocks = SPAN // BLOCK

    def bias_row(bias_rows, h, start):
        step = min(row_width, BLOCK)
        pieces = []
        for first in range(0, BLOCK, step):
            flat = h * length + start + first
            row, col = flat // row_width, flat % row_width
            pieces.append(bias_rows[row : row + 1, col : col + step])
        return jnp.concatenate(pieces, axis=1) if len(pieces) > 1 else pieces[0]

    def tile(source, span, q0, masked):
        k0 = span * SPAN
        key_rows = source[k0 : k0 + SPAN, :width]
        value_rows = source[k0 : k0 + SPAN, width:row_width]
        bias_rows = source[length : length + BIAS_ROWS, :].astype(jnp.float32)
        gathered = None
        for h in range(heads):
            query = q_ref[h, pl.ds(q0, QUERY_ROWS), :]
            later = jnp.zeros((QUERY_ROWS, 1), jnp.float32)
            weights = [None] * tile_blocks
            for block in reversed(range(tile_blocks)):
                b0 = block * BLOCK
                scores = lax.dot_general(
                    query,
                    key_rows[b0 : b0 + BLOCK],
                    (((1,), (1,)), ((), ())),
                    preferred_element_type=jnp.float32,
                )
                scores = scores + bias_row(bias_rows, h, k0 + b0)
                soft = jnp.maximum(scores, 0.0) + jnp.log(1.0 + jnp.exp(-jnp.abs(scores)))
                rest = scores - soft
                if masked:
                    q_pos = q0 - k0 + lax.broadcasted_iota(jnp.int32, scores.shape, 0)
                    k_pos = b0 + lax.broadcasted_iota(jnp.int32, scores.shape, 1)
                    earlier = k_pos < q_pos
                    soft = jnp.where(earlier, soft, 0.0)
                high = soft.astype(jnp.bfloat16)
                low = (soft - high.astype(jnp.float32)).astype(jnp.bfloat16)
                beyond = jnp.dot(high, tri[...], preferred_element_type=jnp.float32) + jnp.dot(
                    low, tri[...], preferred_element_type=jnp.float32
                )
                beyond = beyond + later
                piece = jnp.exp(rest - beyond)
                if masked:
                    piece = jnp.where(earlier, piece, 0.0)
                weights[block] = piece.astype(jnp.bfloat16)
                later = beyond[:, :1] + soft[:, :1]
            joined = jnp.concatenate(weights, axis=1)
            span_out = jnp.dot(joined, value_rows, preferred_element_type=jnp.float32)
            rows = pl.ds(q0, QUERY_ROWS)
            held_after = after[h, rows, :]
            span_out = jnp.exp(-held_after[:, :width]) * span_out
            after[h, rows, :] = held_after + later
            if gathered is None:
                gathered = span_out
            else:
                gathered = jnp.where(lane >= h * HEAD_DIM, span_out, gathered)
        rows = pl.ds(q0, QUERY_ROWS)
        total[rows, :] = total[rows, :] + gathered

    span_count = length // SPAN

    def compute(source, own):
        def chunk(c, carry):
            q0 = pl.multiple_of(c * QUERY_ROWS, QUERY_ROWS)
            for span in reversed(range(span_count)):
                if own:
                    span_of = q0 // SPAN
                    pl.when(span_of == span)(lambda: tile(source, span, q0, True))
                    if span < span_count - 1:
                        pl.when(span_of > span)(lambda: tile(source, span, q0, False))
                else:
                    tile(source, span, q0, False)
            return carry

        lax.fori_loop(0, length // QUERY_ROWS, chunk, 0)

    send(0, own_ref)
    compute(own_ref, True)

    def arrive(d, carry):
        pltpu.make_async_remote_copy(
            src_ref=held.at[d],
            dst_ref=held.at[d],
            send_sem=up_sem.at[d],
            recv_sem=recv_sem.at[d],
            device_id={"sp": partner},
            device_id_type=MESH,
        ).wait_recv()
        pl.when(lax.rem(d, 2) == 0)(lambda: send(d, held.at[d]))
        compute(held.at[d], False)
        return carry

    lax.fori_loop(1, me + 1, arrive, 0)
    out_ref[...] = total[...].astype(jnp.bfloat16)

    def sent(d, source):
        pl.when(has_up)(lambda: up(d, source).wait_send())
        pl.when(odd == 0)(lambda: side(d, d + 1, source).wait_send())
        pl.when((odd == 1) & (d >= 2))(lambda: side(d, d - 1, source).wait_send())

    sent(0, own_ref)

    def drain(half, carry):
        sent(2 * half, held.at[2 * half])
        return carry

    lax.fori_loop(1, me // 2 + 1, drain, 0)


def attend(queries, keys, values, key_bias):
    n = lax.axis_size("sp")
    length = queries.shape[0]
    heads = key_bias.shape[1]
    width = heads * HEAD_DIM
    row_width = 2 * width
    head_of = lax.iota(jnp.int32, width) // HEAD_DIM
    scaled = queries * jnp.bfloat16(HEAD_DIM ** (-0.5))
    per_head = jnp.where(
        head_of[None, None, :] == lax.iota(jnp.int32, heads)[:, None, None],
        scaled[None],
        jnp.bfloat16(0),
    )
    bias_rows = jnp.transpose(key_bias).reshape(-1, row_width)
    bias_rows = jnp.pad(bias_rows, ((0, BIAS_ROWS - bias_rows.shape[0]), (0, 0)))
    own = jnp.concatenate([jnp.concatenate([keys, values], axis=1), bias_rows], axis=0)
    vmem = pl.BlockSpec(memory_space=pltpu.VMEM)
    return pl.pallas_call(
        functools.partial(attend_kernel, n, length, heads),
        out_shape=jax.ShapeDtypeStruct((length, width), jnp.bfloat16),
        in_specs=[vmem, vmem],
        out_specs=vmem,
        scratch_shapes=[
            pltpu.VMEM((n, length + BIAS_ROWS, row_width), jnp.bfloat16),
            pltpu.VMEM((length, width), jnp.float32),
            pltpu.VMEM((heads, length, 128), jnp.float32),
            pltpu.VMEM((BLOCK, BLOCK), jnp.bfloat16),
            pltpu.SemaphoreType.DMA((n + 2,)),
            pltpu.SemaphoreType.DMA((n + 2,)),
            pltpu.SemaphoreType.DMA((n + 2,)),
        ],
        compiler_params=pltpu.CompilerParams(
            collective_id=0, has_side_effects=True, vmem_limit_bytes=40 * 1024 * 1024
        ),
        name="attend",
    )(per_head, own)


def shards(
    queries,
    keys,
    values,
    key_bias,
    residual,
    out_weight,
    norm_gain,
    routes,
    route_weights,
    gate_weight,
    up_weight,
    down_weight,
):
    sp_count = lax.axis_size("sp")
    attended = attend(queries, keys, values, key_bias)
    token_heads = lax.all_to_all(attended, "tp", split_axis=0, concat_axis=1, tiled=True)
    projected = jnp.dot(token_heads, out_weight, preferred_element_type=jnp.float32)
    stream = (residual.astype(jnp.float32) + projected).astype(jnp.bfloat16).astype(jnp.float32)
    normed = (
        stream * lax.rsqrt(jnp.mean(stream * stream, axis=-1, keepdims=True) + epsilon) * norm_gain
    ).astype(jnp.bfloat16)
    token_count = residual.shape[0]
    width_model = residual.shape[1]
    capacity = max(2, 5 * token_count * TOP // (4 * sp_count))
    flat_routes = routes.reshape(-1)
    onehot = (flat_routes[:, None] == lax.iota(jnp.int32, sp_count)[None, :]).astype(jnp.int32)
    before = jnp.cumsum(onehot, axis=0) - onehot
    slot_of = flat_routes * capacity + jnp.sum(before * onehot, axis=1)
    select = (slot_of[:, None] == lax.iota(jnp.int32, sp_count * capacity)[None, :]).astype(
        jnp.bfloat16
    )
    placing = jnp.sum(select.reshape(token_count, TOP, sp_count * capacity), axis=1)
    outgoing = jnp.einsum("ts,td->sd", placing, normed, preferred_element_type=jnp.float32).astype(
        jnp.bfloat16
    )
    arrived = lax.all_to_all(outgoing, "sp", split_axis=0, concat_axis=0, tiled=True)
    row_block = lax.all_gather(arrived, "tp", axis=0, tiled=True)
    gate_act = jnp.dot(row_block, gate_weight[0], preferred_element_type=jnp.float32)
    up_act = jnp.dot(row_block, up_weight[0], preferred_element_type=jnp.float32)
    hidden = (jax.nn.silu(gate_act) * up_act).astype(jnp.bfloat16)
    partial_value = jnp.dot(hidden, down_weight[0], preferred_element_type=jnp.float32)
    summed = lax.psum_scatter(
        lax.optimization_barrier(partial_value.astype(jnp.bfloat16))
        .astype(jnp.float32)
        .astype(jnp.bfloat16),
        "tp",
        scatter_dimension=0,
        tiled=True,
    )
    returned = lax.all_to_all(summed, "sp", split_axis=0, concat_axis=0, tiled=True)
    picked = jnp.dot(select, returned, preferred_element_type=jnp.float32).reshape(
        token_count, TOP, width_model
    )
    routed = jnp.sum(picked * route_weights[:, :, None], axis=1)
    return (stream + routed).astype(jnp.bfloat16)


def solution(mesh):
    return jax.shard_map(
        shards,
        mesh=mesh,
        in_specs=(
            P("sp", "tp"),
            P("sp", "tp"),
            P("sp", "tp"),
            P("sp", "tp"),
            P(("sp", "tp"), None),
            P(),
            P(),
            P(("sp", "tp"), None),
            P(("sp", "tp"), None),
            P("sp", None, "tp"),
            P("sp", None, "tp"),
            P("sp", "tp", None),
        ),
        out_specs=P(("sp", "tp"), None),
        check_vma=False,
    )
```

time: 489 us -> 285 us (0.58)
  blocking collectives: 255 us -> 128 us
  waiting for transfers between devices: 144 us -> 92.1 us
  local copies, waits for them, and re-layouts: 18.3 us -> 3.1 us
  other arithmetic: 19.2 us -> 4.36 us
  Pallas kernels: 0 us -> 9.12 us
    all_to_all x1, blocking collectives: 190 us -> 90.9 us  [shards(): lax.all_to_all(outgoing, 'sp', split_axis=0, concat_axis=0, tiled=True)]
    all_gather x2 -> x0, waiting for transfers between devices: 49.5 us -> none  [the longest x1 40.3 us: shards(): value_piece = lax.all_gather(values, 'sp', axis=0, tiled=True)]
    all_gather x1 -> x0, blocking collectives: 28.3 us -> none  [shards(): bias_piece = lax.all_gather(key_bias, 'sp', axis=0, tiled=True)]
    another operation x6 -> x2, other arithmetic: 12.2 us -> 0.62 us
    pallas_call x0 -> x1, Pallas kernels: none -> 9.12 us  [attend(): pl.pallas_call(functools.partial(attend_kernel, n, length, heads), out_sh...]
    dynamic_update_slice x16 -> x0, local copies, waits for them, and re-layouts: 5.94 us -> none  [the longest x8 5.84 us: place_span(): lax.dynamic_update_index_in_dim(outs_held, span_out, slot, 0)]
  transfers between devices with their start and end apart: 5 -> 3, of which waited for: 5 -> 3; matrix products, arithmetic and copies ran while one was open for 1% -> 1% of each run, Pallas kernels for 0% -> 0%
where the time goes in v1:
time: 285 us; the launch traced here: 284 us
  blocking collectives  128 us (45%)
  waiting for transfers between devices  92.1 us (32%)
  matrix products  31.1 us (11%)
  between operations  13.5 us (5%)
  Pallas kernels  9.12 us (3%)
  other arithmetic  4.36 us (2%)
  starting transfers between devices  3.41 us (1%)
  local copies, waits for them, and re-layouts  3.1 us (1%)
    all_to_all x1, blocking collectives, shards(): lax.all_to_all(outgoing, 'sp', split_axis=0, concat_axis=0, tiled=True)  90.9 us
    reduce_scatter x1, waiting for transfers between devices, shards(): lax.psum_scatter(lax.optimization_barrier(partial_value.astype(jnp.bfloat...  51.5 us
    all_gather x1, waiting for transfers between devices, shards(): row_block = lax.all_gather(arrived, 'tp', axis=0, tiled=True)  39.1 us
    all_to_all x1, blocking collectives, shards(): lax.all_to_all(summed, 'sp', split_axis=0, concat_axis=0, tiled=True)  36.7 us
    dot_general x1, matrix products, shards(): jnp.dot(hidden, down_weight[0], preferred_element_type=jnp.float32)  17.9 us
    dot_general x1, matrix products, shards(): jnp.dot(row_block, gate_weight[0], preferred_element_type=jnp.float32)  10.2 us
    pallas_call x1, Pallas kernels, attend(): pl.pallas_call(functools.partial(attend_kernel, n, length, heads), out_sh...  9.12 us
  transfers between devices with their start and end apart: 3, of which 3 were waited for; matrix products, arithmetic and copies ran while one was open for 1% of the time, Pallas kernels for 0%

profile of v1, /device:TPU:0, one launch (start us, length us, event | category | flops | bytes accessed | tf_op | source)
XLA Modules:
  0.0 284.3 jit_solution(4584275443465113624)
XLA Ops:
  6.6 0.8 reshape.115
  7.4 0.9 broadcast_multiply_fusion
  8.3 1.0 fusion.15.own_ref
  9.3 9.1 %attend.1 = bf16[512,128]{1,0:T(8,128)(2,1)S(1)} custom-call(bf16[2,512,128]{2,1,0:T(8,128)(2,1)S(1)} %broadcast_select_fusion.q_ref, bf16[528,256]{1,0:T(8,128)(2,1)S(1)} %fusion.15.own_ref), custom_call_target="tpu_custom_call" | custom-call | tf_op jit(solution)/shard_map/attend/pallas_call | solution.py:203
  18.5 0.8 copy.27
  19.2 3.3 %all-to-all-start = ((bf16[4,128,128]{1,2,0:T(8,128)(2,1)}), bf16[4,128,128]{1,2,0:T(8,128)(2,1)S(1)}, u32[]{:S(2)}, u32[]{:S(2)}) async-start(bf16[4,128,128]{1,2,0:T(8,128)(2,1)} %copy.27), calls=%async_computation | async-start | bytes 262144 | tf_op jit(solution)/shard_map/all_to_all | solution.py:240
  22.6 0.0 all-gather.2.cloned.1.call-start
  22.6 0.8 copy.28
  23.4 0.1 eq.86
  23.6 0.1 eq.82
  23.7 0.6 reduce-window.6
  24.3 0.2 slice_reduce_fusion
  24.6 0.1 fusion.19
  24.6 0.1 reduce_sum.42
  24.8 0.1 copy.30
  24.9 0.7 multiply_add_fusion
  25.6 1.5 all-to-all-done
  27.1 0.0 copy-done
  27.1 1.6 multiply_reduce_fusion
  28.8 0.6 convolution_convert_fusion.1
  29.3 90.9 %all_to_all.43 = bf16[8,40,2048]{2,1,0:T(8,128)(2,1)} all-to-all(bf16[8,40,2048]{2,1,0:T(8,128)(2,1)S(1)} %bitcast.41), channel_id=1, replica_groups=mesh['sp'=8,'tp'=4] {'sp'}, dimensions={0} | all-to-all | bytes 2621440 | tf_op jit(solution)/shard_map/all_to_all | solution.py:260
  120.2 0.0 all-gather.2.cloned.1.call-update
  120.3 0.0 reduce-scatter.2.cloned.1.call-start
  120.3 39.1 %all-gather.2.cloned.1.call-done = bf16[1280,2048]{1,0:T(8,128)(2,1)} async-done(((bf16[320,2048]{1,0:T(8,128)(2,1)}), bf16[1280,2048]{1,0:T(8,128)(2,1)}) %all-gather.2.cloned.1.call-update) | async-done | bytes 5242896 | tf_op jit(solution)/shard_map/all_gather | solution.py:261
  159.4 10.2 %fusion.2 = f32[1280,1024]{1,0:T(8,128)} fusion(bf16[1280,2048]{1,0:T(8,128)(2,1)} %all-gather.2.cloned.1.call-done, bf16[1,2048,1024]{2,1,0:T(8,128)(2,1)} %param.21), kind=kOutput, calls=%fused_computation.4 | convolution fusion | flops 5368709120 | bytes 14680064 | tf_op jit(solution)/shard_map/dot_general | solution.py:262
  169.6 17.9 %convolution_convert_fusion = bf16[1280,2048]{1,0:T(8,128)(2,1)} fusion(bf16[1,1024,2048]{2,1,0:T(8,128)(2,1)} %param.23, f32[1280,1024]{1,0:T(8,128)} %fusion.2, bf16[1280,2048]{1,0:T(8,128)(2,1)} %all-gather.2.cloned.1.call-done, bf16[1,2048,1024]{2,1,0:T(8,128)(2,1)} %param.22), kind=kOutput, calls=%fused_computation | convolution fusion | flops 10747904000 | bytes 24117248 | tf_op jit(solution)/shard_map/dot_general | solution.py:265
  187.5 0.0 reduce-scatter.2.cloned.1.call-update
  187.5 51.5 %reduce-scatter.2.cloned.1.call-done = bf16[320,2048]{1,0:T(8,128)(2,1)} async-done(((bf16[1280,2048]{1,0:T(8,128)(2,1)}), bf16[320,2048]{1,0:T(8,128)(2,1)}) %reduce-scatter.2.cloned.1.call-update) | async-done | bytes 1310736 | tf_op jit(solution)/shard_map/reduce_scatter | solution.py:266
  239.0 36.7 %all_to_all.44 = bf16[8,40,2048]{2,1,0:T(8,128)(2,1)S(1)} all-to-all(bf16[8,40,2048]{2,1,0:T(8,128)(2,1)} %bitcast.42), channel_id=1, replica_groups=mesh['sp'=8,'tp'=4] {'sp'}, dimensions={0} | all-to-all | bytes 2621440 | tf_op jit(solution)/shard_map/all_to_all | solution.py:274
  275.7 0.0 copy-done.2
  275.8 0.8 fusion.8
  276.5 0.9 add_convert_fusion
  (12 shorter events, 0.1 us)
Async XLA Ops:
  6.5 20.6 %copy-start = (bf16[512,2048]{1,0:T(8,128)(2,1)S(1)}, bf16[512,2048]{1,0:T(8,128)(2,1)}, u32[]{:S(2)}) copy-start(bf16[512,2048]{1,0:T(8,128)(2,1)} %param.17) | copy-start | bytes 6291460
  6.5 22.2 %copy-start.1 = (f32[2048]{0:T(1024)S(1)}, f32[2048]{0:T(1024)}, u32[]{:S(2)}) copy-start(f32[2048]{0:T(1024)} %param.18) | copy-start | bytes 24580
  19.2 7.9 %all-to-all-start = ((bf16[4,128,128]{1,2,0:T(8,128)(2,1)}), bf16[4,128,128]{1,2,0:T(8,128)(2,1)S(1)}, u32[]{:S(2)}, u32[]{:S(2)}) async-start(bf16[4,128,128]{1,2,0:T(8,128)(2,1)} %copy.27), calls=%async_computation | async-start | bytes 262144 | tf_op jit(solution)/shard_map/all_to_all | solution.py:240
  22.6 136.8 %all-gather.2.cloned.1.call-start = ((), (), s32[]{:S(2)}) async-start(), calls=%async_computation.4 | async-start | bytes 6553600 | tf_op jit(solution)/shard_map/all_gather | solution.py:261
  120.3 118.8 %reduce-scatter.2.cloned.1.call-start = ((), (), s32[]{:S(2)}) async-start(), calls=%async_computation.5 | async-start | bytes 6553600 | tf_op jit(solution)/shard_map/reduce_scatter | solution.py:266
  187.5 88.2 %copy-start.2 = (f32[128,2]{0,1:T(2,128)S(1)}, f32[128,2]{0,1:T(2,128)}, u32[]{:S(2)}) copy-start(f32[128,2]{0,1:T(2,128)} %param.20) | copy-start | bytes 3076
Sparse Core Ops, SparseCore 0:
  120.4 38.9 all-gather.1
  187.7 51.3 reduce-scatter.1

commit v2 on v1

--- a/solution.py
+++ b/solution.py
@@ -221,6 +221,267 @@
     )(per_head, own)
 
 
+def dispatch_kernel(n, groups, outgoing, rows, sp_sem, chip_sem, core_sem, recv_sem):
+    me, my_t = lax.axis_index("sp"), lax.axis_index("tp")
+    mate = my_t + 1 - 2 * lax.rem(my_t, 2)
+    chips = groups // 2
+    alike = [lax.rem(my_t + 2 * k, groups) for k in range(1, chips)]
+    greet_all(n, me, mate, alike)
+
+    def copy(source, t, s, send_sem, device):
+        return pltpu.make_async_remote_copy(
+            src_ref=source,
+            dst_ref=rows.at[t * n + s],
+            send_sem=send_sem,
+            recv_sem=recv_sem.at[t * n + s],
+            device_id=device,
+            device_id_type=MESH,
+        )
+
+    def to_expert(r):
+        target = lax.rem(me + r, n)
+        return copy(outgoing.at[target], my_t, me, sp_sem.at[r], {"sp": target})
+
+    def to_chip(k, s, source):
+        return copy(source, my_t, s, chip_sem.at[k * n + s], {"tp": alike[k]})
+
+    def to_mate(t, s, source):
+        return copy(source, t, s, core_sem.at[t * n + s], {"tp": mate})
+
+    def arrived(t, s):
+        copy(rows.at[t * n + s], t, s, core_sem.at[t * n + s], {"tp": mate}).wait_recv()
+
+    def spread(s, source):
+        for k in range(chips - 1):
+            to_chip(k, s, source).start()
+        to_mate(my_t, s, source).start()
+
+    def relay(r):
+        s = lax.rem(me + n - r, n)
+        for t in alike:
+            arrived(t, s)
+            to_mate(t, s, rows.at[t * n + s]).start()
+
+    def issue(r, carry):
+        to_expert(r).start()
+        return carry
+
+    spread(me, outgoing.at[me])
+    lax.fori_loop(1, n, issue, 0)
+    rows[my_t * n + me] = outgoing[me]
+
+    def step(r, carry):
+        s = lax.rem(me + n - r, n)
+        arrived(my_t, s)
+        spread(s, rows.at[my_t * n + s])
+        relay(r - 1)
+        return carry
+
+    lax.fori_loop(1, n, step, 0)
+    relay(n - 1)
+
+    def finish(s, carry):
+        arrived(mate, s)
+        for t in alike:
+            arrived(t + 1 - 2 * lax.rem(t, 2), s)
+        pl.when(s >= 1)(lambda: to_expert(s).wait_send())
+        for k in range(chips - 1):
+            to_chip(k, s, outgoing.at[me]).wait_send()
+            to_mate(alike[k], s, outgoing.at[me]).wait_send()
+        to_mate(my_t, s, outgoing.at[me]).wait_send()
+        return carry
+
+    lax.fori_loop(0, n, finish, 0)
+
+
+def greet_all(n, me, mate, alike):
+    barrier = pltpu.get_barrier_semaphore()
+
+    def greet(device):
+        pl.semaphore_signal(barrier, inc=1, device_id=device, device_id_type=MESH)
+
+    def greet_sp(r, carry):
+        greet({"sp": lax.rem(me + r, n)})
+        return carry
+
+    lax.fori_loop(1, n, greet_sp, 0)
+    greet({"tp": mate})
+    for t in alike:
+        greet({"tp": t})
+    pl.semaphore_wait(barrier, n + len(alike))
+
+
+def combine_kernel(
+    n, groups, partial, back, pair, other, done, pair_send, pair_recv, chip_send, chip_recv,
+    back_send, back_recv,
+):
+    me, my_t = lax.axis_index("sp"), lax.axis_index("tp")
+    core = lax.rem(my_t, 2)
+    mate = my_t + 1 - 2 * core
+    chips = groups // 2
+    alike = [lax.rem(my_t + 2 * k, groups) for k in range(1, chips)]
+    greet_all(n, me, mate, alike)
+
+    def home(r):
+        return lax.rem(me + 1 + r, n)
+
+    def pair_copy(chip, r):
+        return pltpu.make_async_remote_copy(
+            src_ref=partial.at[(2 * chip + 1 - core) * n + home(r)],
+            dst_ref=pair.at[chip * n + r],
+            send_sem=pair_send.at[chip * n + r],
+            recv_sem=pair_recv.at[chip * n + r],
+            device_id={"tp": mate},
+            device_id_type=MESH,
+        )
+
+    def chip_copy(k, r):
+        return pltpu.make_async_remote_copy(
+            src_ref=pair.at[(alike[k] // 2) * n + r],
+            dst_ref=other.at[k * n + r],
+            send_sem=chip_send.at[k * n + r],
+            recv_sem=chip_recv.at[k * n + r],
+            device_id={"tp": alike[k]},
+            device_id_type=MESH,
+        )
+
+    def back_copy(r):
+        return pltpu.make_async_remote_copy(
+            src_ref=done.at[r],
+            dst_ref=back.at[me],
+            send_sem=back_send.at[r],
+            recv_sem=back_recv.at[me],
+            device_id={"sp": home(r)},
+            device_id_type=MESH,
+        )
+
+    def start_pairs(r, carry):
+        for chip in range(chips):
+            pair_copy(chip, r).start()
+        return carry
+
+    lax.fori_loop(0, n, start_pairs, 0)
+
+    def add_pairs(r):
+        for chip in range(chips):
+            pair_copy(chip, r).wait_recv()
+        for k in range(chips - 1):
+            chip = alike[k] // 2
+            pair[chip * n + r] = (
+                partial[alike[k] * n + home(r)].astype(jnp.float32)
+                + pair[chip * n + r].astype(jnp.float32)
+            ).astype(jnp.bfloat16)
+
+    def add_chips(r):
+        value = partial[my_t * n + home(r)].astype(jnp.float32) + pair[
+            (my_t // 2) * n + r
+        ].astype(jnp.float32)
+        for k in range(chips - 1):
+            chip_copy(k, r).wait_recv()
+            value = value + other[k * n + r].astype(jnp.float32)
+        return value.astype(jnp.bfloat16)
+
+    def send_chips(r):
+        for k in range(chips - 1):
+            chip_copy(k, r).start()
+
+    lag = 1
+    for r in range(lag):
+        add_pairs(r)
+        send_chips(r)
+
+    def step(r, carry):
+        add_pairs(r)
+        send_chips(r)
+        done[r - lag] = add_chips(r - lag)
+        back_copy(r - lag).start()
+        return carry
+
+    lax.fori_loop(lag, n, step, 0)
+    for r in range(n - lag, n):
+        if r == n - 1:
+            back[me] = add_chips(r)
+        else:
+            done[r] = add_chips(r)
+            back_copy(r).start()
+
+    def finish(r, carry):
+        for chip in range(chips):
+            pair_copy(chip, r).wait_send()
+        for k in range(chips - 1):
+            chip_copy(k, r).wait_send()
+        return carry
+
+    lax.fori_loop(0, n, finish, 0)
+
+    def finish_back(r, carry):
+        back_copy(r).wait_send()
+        source = home(r)
+        pltpu.make_async_remote_copy(
+            src_ref=done.at[r],
+            dst_ref=back.at[source],
+            send_sem=back_send.at[r],
+            recv_sem=back_recv.at[source],
+            device_id={"sp": source},
+            device_id_type=MESH,
+        ).wait_recv()
+        return carry
+
+    lax.fori_loop(0, n - 1, finish_back, 0)
+
+
+def dispatch(outgoing):
+    n, groups = lax.axis_size("sp"), lax.axis_size("tp")
+    chips = groups // 2
+    _, capacity, width = outgoing.shape
+    vmem = pl.BlockSpec(memory_space=pltpu.VMEM)
+    return pl.pallas_call(
+        functools.partial(dispatch_kernel, n, groups),
+        out_shape=jax.ShapeDtypeStruct((groups * n, capacity, width), outgoing.dtype),
+        in_specs=[vmem],
+        out_specs=vmem,
+        scratch_shapes=[
+            pltpu.SemaphoreType.DMA((n,)),
+            pltpu.SemaphoreType.DMA((max(1, chips - 1) * n,)),
+            pltpu.SemaphoreType.DMA((groups * n,)),
+            pltpu.SemaphoreType.DMA((groups * n,)),
+        ],
+        compiler_params=pltpu.CompilerParams(
+            collective_id=1, has_side_effects=True, vmem_limit_bytes=56 * 1024 * 1024
+        ),
+        name="dispatch",
+    )(outgoing)
+
+
+def combine(partial):
+    n, groups = lax.axis_size("sp"), lax.axis_size("tp")
+    chips = groups // 2
+    _, capacity, width = partial.shape
+    vmem = pl.BlockSpec(memory_space=pltpu.VMEM)
+    apart = max(1, chips - 1) * n
+    return pl.pallas_call(
+        functools.partial(combine_kernel, n, groups),
+        out_shape=jax.ShapeDtypeStruct((n, capacity, width), partial.dtype),
+        in_specs=[vmem],
+        out_specs=vmem,
+        scratch_shapes=[
+            pltpu.VMEM((chips * n, capacity, width), partial.dtype),
+            pltpu.VMEM((apart, capacity, width), partial.dtype),
+            pltpu.VMEM((n, capacity, width), partial.dtype),
+            pltpu.SemaphoreType.DMA((chips * n,)),
+            pltpu.SemaphoreType.DMA((chips * n,)),
+            pltpu.SemaphoreType.DMA((apart,)),
+            pltpu.SemaphoreType.DMA((apart,)),
+            pltpu.SemaphoreType.DMA((n,)),
+            pltpu.SemaphoreType.DMA((n,)),
+        ],
+        compiler_params=pltpu.CompilerParams(
+            collective_id=2, has_side_effects=True, vmem_limit_bytes=56 * 1024 * 1024
+        ),
+        name="combine",
+    )(partial)
+
+
 def shards(
     queries,
     keys,
@@ -257,21 +518,14 @@
     outgoing = jnp.einsum("ts,td->sd", placing, normed, preferred_element_type=jnp.float32).astype(
         jnp.bfloat16
     )
-    arrived = lax.all_to_all(outgoing, "sp", split_axis=0, concat_axis=0, tiled=True)
-    row_block = lax.all_gather(arrived, "tp", axis=0, tiled=True)
+    row_block = dispatch(outgoing.reshape(sp_count, capacity, width_model)).reshape(-1, width_model)
     gate_act = jnp.dot(row_block, gate_weight[0], preferred_element_type=jnp.float32)
     up_act = jnp.dot(row_block, up_weight[0], preferred_element_type=jnp.float32)
     hidden = (jax.nn.silu(gate_act) * up_act).astype(jnp.bfloat16)
     partial_value = jnp.dot(hidden, down_weight[0], preferred_element_type=jnp.float32)
-    summed = lax.psum_scatter(
-        lax.optimization_barrier(partial_value.astype(jnp.bfloat16))
-        .astype(jnp.float32)
-        .astype(jnp.bfloat16),
-        "tp",
-        scatter_dimension=0,
-        tiled=True,
-    )
-    returned = lax.all_to_all(summed, "sp", split_axis=0, concat_axis=0, tiled=True)
+    returned = combine(
+        partial_value.astype(jnp.bfloat16).reshape(-1, capacity, width_model)
+    ).reshape(-1, width_model)
     picked = jnp.dot(select, returned, preferred_element_type=jnp.float32).reshape(
         token_count, TOP, width_model
     )

time: 285 us -> 207 us (0.73)
  Pallas kernels: 9.12 us -> 160 us
  blocking collectives: 128 us -> 0 us
  waiting for transfers between devices: 92.1 us -> 1.41 us
  between operations: 13.5 us -> 0.13 us
    pallas_call x0 -> x2, Pallas kernels: none -> 151 us  [the longest x1 101 us: dispatch(): pl.pallas_call(functools.partial(dispatch_kernel, n, groups), out_shape=j...]
    all_to_all x2 -> x0, blocking collectives: 128 us -> none  [the longest x1 90.9 us: shards(): lax.all_to_all(outgoing, 'sp', split_axis=0, concat_axis=0, tiled=True)]
    reduce_scatter x1 -> x0, waiting for transfers between devices: 51.5 us -> none  [shards(): lax.psum_scatter(lax.optimization_barrier(partial_value.astype(jnp.bfloat...]
    all_gather x1 -> x0, waiting for transfers between devices: 39.1 us -> none  [shards(): row_block = lax.all_gather(arrived, 'tp', axis=0, tiled=True)]
  transfers between devices with their start and end apart: 3 -> 1, of which waited for: 3 -> 1; matrix products, arithmetic and copies ran while one was open for 1% -> 1% of each run, Pallas kernels for 0% -> 0%
where the time goes in v2:
time: 207 us; the launch traced here: 205 us
  Pallas kernels  160 us (77%)
  matrix products  32.4 us (16%)
  other arithmetic  4.36 us (2%)
  starting transfers between devices  3.51 us (2%)
  local copies, waits for them, and re-layouts  3.11 us (2%)
    pallas_call x1, Pallas kernels, dispatch(): pl.pallas_call(functools.partial(dispatch_kernel, n, groups), out_shape=j...  101 us
    pallas_call x1, Pallas kernels, combine(): pl.pallas_call(functools.partial(combine_kernel, n, groups), out_shape=ja...  50 us
    dot_general x1, matrix products, shards(): jnp.dot(hidden, down_weight[0], preferred_element_type=jnp.float32)  18 us
    pallas_call x1, Pallas kernels, attend(): pl.pallas_call(functools.partial(attend_kernel, n, length, heads), out_sh...  9.13 us
    dot_general x1, matrix products, shards(): jnp.dot(row_block, gate_weight[0], preferred_element_type=jnp.float32)  9.06 us
  transfers between devices with their start and end apart: 1, of which 1 were waited for; matrix products, arithmetic and copies ran while one was open for 1% of the time, Pallas kernels for 0%

profile of v2, /device:TPU:0, one launch (start us, length us, event | category | flops | bytes accessed | tf_op | source)
XLA Modules:
  0.0 205.4 jit_solution(7173207963141675265)
XLA Ops:
  0.0 0.0 copy-start
  0.0 0.0 copy-start.1
  0.0 0.8 reshape.123
  0.9 0.9 broadcast_multiply_fusion
  1.8 1.0 fusion.15.own_ref
  2.8 9.1 %attend.1 = bf16[512,128]{1,0:T(8,128)(2,1)S(1)} custom-call(bf16[2,512,128]{2,1,0:T(8,128)(2,1)S(1)} %broadcast_select_fusion.q_ref, bf16[528,256]{1,0:T(8,128)(2,1)S(1)} %fusion.15.own_ref), custom_call_target="tpu_custom_call" | custom-call | tf_op jit(solution)/shard_map/attend/pallas_call | solution.py:203
  11.9 0.8 copy.27
  12.7 3.5 %all-to-all-start = ((bf16[4,128,128]{1,2,0:T(8,128)(2,1)}), bf16[4,128,128]{1,2,0:T(8,128)(2,1)S(1)}, u32[]{:S(2)}, u32[]{:S(2)}) async-start(bf16[4,128,128]{1,2,0:T(8,128)(2,1)} %copy.27), calls=%async_computation | async-start | bytes 262144 | tf_op jit(solution)/shard_map/all_to_all | solution.py:501
  16.2 0.8 copy.28
  17.0 0.1 eq.86
  17.2 0.1 eq.82
  17.3 0.6 reduce-window.6
  17.9 0.2 slice_reduce_fusion
  18.2 0.1 fusion.19
  18.3 0.1 reduce_sum.42
  18.4 0.1 copy.30
  18.5 0.7 multiply_add_fusion
  19.2 1.4 all-to-all-done
  20.6 0.0 copy-done
  20.6 1.6 multiply_reduce_fusion
  22.2 0.0 copy-done.1
  22.2 0.0 copy-start.2
  22.2 1.7 convolution_convert_fusion.1
  23.9 101.3 %dispatch.1 = bf16[32,40,2048]{2,1,0:T(8,128)(2,1)} custom-call(bf16[8,40,2048]{2,1,0:T(8,128)(2,1)} %bitcast.43), custom_call_target="tpu_custom_call" | custom-call | tf_op jit(solution)/shard_map/dispatch/pallas_call | solution.py:438
  125.2 0.0 copy-done.2
  125.3 9.1 %fusion.2 = f32[1280,1024]{1,0:T(8,128)} fusion(bf16[1280,2048]{1,0:T(8,128)(2,1)} %bitcast.40, bf16[1,2048,1024]{2,1,0:T(8,128)(2,1)S(1)} %copy-done.2), kind=kOutput, calls=%fused_computation.4 | convolution fusion | flops 5368709120 | bytes 14680064 | tf_op jit(solution)/shard_map/dot_general | solution.py:522
  134.3 18.0 %convolution_convert_fusion = bf16[1280,2048]{1,0:T(8,128)(2,1)} fusion(bf16[1,1024,2048]{2,1,0:T(8,128)(2,1)} %param.23, f32[1280,1024]{1,0:T(8,128)} %fusion.2, bf16[1280,2048]{1,0:T(8,128)(2,1)} %bitcast.41, bf16[1,2048,1024]{2,1,0:T(8,128)(2,1)} %param.22), kind=kOutput, calls=%fused_computation | convolution fusion | flops 10747904000 | bytes 24117248 | tf_op jit(solution)/shard_map/dot_general | solution.py:525
  152.3 0.0 copy-start.3
  152.3 50.0 %combine.1 = bf16[8,40,2048]{2,1,0:T(8,128)(2,1)} custom-call(bf16[32,40,2048]{2,1,0:T(8,128)(2,1)} %bitcast.42), custom_call_target="tpu_custom_call" | custom-call | tf_op jit(solution)/shard_map/combine/pallas_call | solution.py:462
  202.3 0.0 copy-done.3
  202.3 2.2 %fusion.8 = f32[128,2048]{1,0:T(8,128)S(1)} fusion(bf16[320,2048,1]{1,0,2:T(8,128)(2,1)} %bitcast.44, f32[128,2]{0,1:T(2,128)S(1)} %copy-done.3, s32[128,2]{0,1:T(2,128)S(1)} %multiply_add_fusion), kind=kOutput, calls=%fused_computation.11 | convolution fusion | flops 336412672 | bytes 2361344 | tf_op jit(solution)/shard_map/dot_general | solution.py:529
  204.5 0.9 add_convert_fusion
  (8 shorter events, 0.1 us)
Async XLA Ops:
  0.0 20.6 %copy-start = (bf16[512,2048]{1,0:T(8,128)(2,1)S(1)}, bf16[512,2048]{1,0:T(8,128)(2,1)}, u32[]{:S(2)}) copy-start(bf16[512,2048]{1,0:T(8,128)(2,1)} %param.17) | copy-start | bytes 6291460
  0.0 22.2 %copy-start.1 = (f32[2048]{0:T(1024)S(1)}, f32[2048]{0:T(1024)}, u32[]{:S(2)}) copy-start(f32[2048]{0:T(1024)} %param.18) | copy-start | bytes 24580
  12.7 7.9 %all-to-all-start = ((bf16[4,128,128]{1,2,0:T(8,128)(2,1)}), bf16[4,128,128]{1,2,0:T(8,128)(2,1)S(1)}, u32[]{:S(2)}, u32[]{:S(2)}) async-start(bf16[4,128,128]{1,2,0:T(8,128)(2,1)} %copy.27), calls=%async_computation | async-start | bytes 262144 | tf_op jit(solution)/shard_map/all_to_all | solution.py:501
  22.2 103.0 %copy-start.2 = (bf16[1,2048,1024]{2,1,0:T(8,128)(2,1)S(1)}, bf16[1,2048,1024]{2,1,0:T(8,128)(2,1)}, u32[]{:S(2)}) copy-start(bf16[1,2048,1024]{2,1,0:T(8,128)(2,1)} %param.21) | copy-start | bytes 12582916
  152.3 50.0 %copy-start.3 = (f32[128,2]{0,1:T(2,128)S(1)}, f32[128,2]{0,1:T(2,128)}, u32[]{:S(2)}) copy-start(f32[128,2]{0,1:T(2,128)} %param.20) | copy-start | bytes 3076

commit v3 on v2

--- a/solution.py
+++ b/solution.py
@@ -221,12 +221,23 @@
     )(per_head, own)
 
 
-def dispatch_kernel(n, groups, outgoing, rows, sp_sem, chip_sem, core_sem, recv_sem):
+def dispatch_kernel(
+    n, groups, outgoing, gate_hbm, up_hbm, down_hbm, partial, rows, block, hidden, gate, up, down,
+    weight_sem, sp_sem, chip_sem, core_sem, recv_sem,
+):
     me, my_t = lax.axis_index("sp"), lax.axis_index("tp")
     mate = my_t + 1 - 2 * lax.rem(my_t, 2)
     chips = groups // 2
     alike = [lax.rem(my_t + 2 * k, groups) for k in range(1, chips)]
+    loads = [
+        pltpu.make_async_copy(gate_hbm, gate, weight_sem.at[0]),
+        pltpu.make_async_copy(up_hbm, up, weight_sem.at[1]),
+        pltpu.make_async_copy(down_hbm, down, weight_sem.at[2]),
+    ]
+    for load in loads:
+        load.start()
     greet_all(n, me, mate, alike)
+    capacity = outgoing.shape[1]
 
     def copy(source, t, s, send_sem, device):
         return pltpu.make_async_remote_copy(
@@ -270,20 +281,54 @@
     lax.fori_loop(1, n, issue, 0)
     rows[my_t * n + me] = outgoing[me]
 
+    def expert(r):
+        s = lax.rem(me + n - r, n)
+        arrived(mate, s)
+        for t in alike:
+            arrived(t + 1 - 2 * lax.rem(t, 2), s)
+        block[...] = jnp.concatenate([rows[t * n + s] for t in range(groups)], axis=0)
+
+        def units(f, carry):
+            columns = pl.ds(pl.multiple_of(f * BLOCK, BLOCK), BLOCK)
+            gate_act = jnp.dot(block[...], gate[:, columns], preferred_element_type=jnp.float32)
+            up_act = jnp.dot(block[...], up[:, columns], preferred_element_type=jnp.float32)
+            silu = gate_act / (1.0 + jnp.exp(-gate_act))
+            hidden[:, columns] = (silu * up_act).astype(jnp.bfloat16)
+            return carry
+
+        lax.fori_loop(0, gate.shape[1] // BLOCK, units, 0)
+
+        def features(f, carry):
+            columns = pl.ds(pl.multiple_of(f * BLOCK, BLOCK), BLOCK)
+            value = jnp.dot(hidden[...], down[:, columns], preferred_element_type=jnp.float32)
+            for t in range(groups):
+                piece = value[t * capacity : (t + 1) * capacity]
+                partial[t * n + s, :, columns] = piece.astype(jnp.bfloat16)
+            return carry
+
+        lax.fori_loop(0, down.shape[1] // BLOCK, features, 0)
+
     def step(r, carry):
         s = lax.rem(me + n - r, n)
         arrived(my_t, s)
         spread(s, rows.at[my_t * n + s])
         relay(r - 1)
-        return carry
-
-    lax.fori_loop(1, n, step, 0)
+        pl.when(r >= 2)(lambda: expert(r - 2))
+        return carry
+
+    lax.fori_loop(1, 2, step, 0)
+    for load in loads:
+        load.wait()
+    lax.fori_loop(2, n, step, 0)
     relay(n - 1)
 
+    def last(r, carry):
+        expert(r)
+        return carry
+
+    lax.fori_loop(n - 2, n, last, 0)
+
     def finish(s, carry):
-        arrived(mate, s)
-        for t in alike:
-            arrived(t + 1 - 2 * lax.rem(t, 2), s)
         pl.when(s >= 1)(lambda: to_expert(s).wait_send())
         for k in range(chips - 1):
             to_chip(k, s, outgoing.at[me]).wait_send()
@@ -430,27 +475,36 @@
     lax.fori_loop(0, n - 1, finish_back, 0)
 
 
-def dispatch(outgoing):
+def dispatch(outgoing, gate, up, down):
     n, groups = lax.axis_size("sp"), lax.axis_size("tp")
     chips = groups // 2
     _, capacity, width = outgoing.shape
+    units = gate.shape[1]
     vmem = pl.BlockSpec(memory_space=pltpu.VMEM)
+    anywhere = pl.BlockSpec(memory_space=pl.ANY)
     return pl.pallas_call(
         functools.partial(dispatch_kernel, n, groups),
         out_shape=jax.ShapeDtypeStruct((groups * n, capacity, width), outgoing.dtype),
-        in_specs=[vmem],
+        in_specs=[vmem, anywhere, anywhere, anywhere],
         out_specs=vmem,
         scratch_shapes=[
+            pltpu.VMEM((groups * n, capacity, width), outgoing.dtype),
+            pltpu.VMEM((groups * capacity, width), outgoing.dtype),
+            pltpu.VMEM((groups * capacity, units), outgoing.dtype),
+            pltpu.VMEM((width, units), gate.dtype),
+            pltpu.VMEM((width, units), up.dtype),
+            pltpu.VMEM((units, width), down.dtype),
+            pltpu.SemaphoreType.DMA((3,)),
             pltpu.SemaphoreType.DMA((n,)),
             pltpu.SemaphoreType.DMA((max(1, chips - 1) * n,)),
             pltpu.SemaphoreType.DMA((groups * n,)),
             pltpu.SemaphoreType.DMA((groups * n,)),
         ],
         compiler_params=pltpu.CompilerParams(
-            collective_id=1, has_side_effects=True, vmem_limit_bytes=56 * 1024 * 1024
+            collective_id=1, has_side_effects=True, vmem_limit_bytes=60 * 1024 * 1024
         ),
         name="dispatch",
-    )(outgoing)
+    )(outgoing, gate, up, down)
 
 
 def combine(partial):
@@ -518,14 +572,13 @@
     outgoing = jnp.einsum("ts,td->sd", placing, normed, preferred_element_type=jnp.float32).astype(
         jnp.bfloat16
     )
-    row_block = dispatch(outgoing.reshape(sp_count, capacity, width_model)).reshape(-1, width_model)
-    gate_act = jnp.dot(row_block, gate_weight[0], preferred_element_type=jnp.float32)
-    up_act = jnp.dot(row_block, up_weight[0], preferred_element_type=jnp.float32)
-    hidden = (jax.nn.silu(gate_act) * up_act).astype(jnp.bfloat16)
-    partial_value = jnp.dot(hidden, down_weight[0], preferred_element_type=jnp.float32)
-    returned = combine(
-        partial_value.astype(jnp.bfloat16).reshape(-1, capacity, width_model)
-    ).reshape(-1, width_model)
+    partial_rows = dispatch(
+        outgoing.reshape(sp_count, capacity, width_model),
+        gate_weight[0],
+        up_weight[0],
+        down_weight[0],
+    )
+    returned = combine(partial_rows).reshape(-1, width_model)
     picked = jnp.dot(select, returned, preferred_element_type=jnp.float32).reshape(
         token_count, TOP, width_model
     )

time: 207 us -> 194 us (0.937)
  matrix products: 32.4 us -> 5.42 us
  Pallas kernels: 160 us -> 173 us
    dot_general x2 -> x0, matrix products: 27 us -> none  [the longest x1 18 us: shards(): jnp.dot(hidden, down_weight[0], preferred_element_type=jnp.float32)]
    pallas_call x1, Pallas kernels: 101 us -> 113 us  [dispatch(): pl.pallas_call(functools.partial(dispatch_kernel, n, groups), out_shape=j...]
where the time goes in v3:
time: 194 us; the launch traced here: 191 us
  Pallas kernels  173 us (89%)
  matrix products  5.42 us (3%)
  other arithmetic  3.66 us (2%)
  starting transfers between devices  3.33 us (2%)
  waiting for transfers between devices  2.92 us (2%)
  local copies, waits for them, and re-layouts  2.44 us (1%)
    pallas_call x1, Pallas kernels, dispatch(): pl.pallas_call(functools.partial(dispatch_kernel, n, groups), out_shape=j...  113 us
    pallas_call x1, Pallas kernels, combine(): pl.pallas_call(functools.partial(combine_kernel, n, groups), out_shape=ja...  50.7 us
    pallas_call x1, Pallas kernels, attend(): pl.pallas_call(functools.partial(attend_kernel, n, length, heads), out_sh...  9.12 us
  transfers between devices with their start and end apart: 1, of which 1 were waited for; matrix products, arithmetic and copies ran while one was open for 1% of the time, Pallas kernels for 0%

profile of v3, /device:TPU:0, one launch (start us, length us, event | category | flops | bytes accessed | tf_op | source)
XLA Modules:
  0.0 191.0 jit_solution(699048157853487354)
XLA Ops:
  0.0 0.0 copy-start
  0.0 0.0 copy-start.2
  0.0 0.8 reshape.117
  0.9 0.9 broadcast_multiply_fusion
  1.8 1.0 fusion.9.own_ref
  2.8 9.1 %attend.1 = bf16[512,128]{1,0:T(8,128)(2,1)S(1)} custom-call(bf16[2,512,128]{2,1,0:T(8,128)(2,1)S(1)} %broadcast_select_fusion.q_ref, bf16[528,256]{1,0:T(8,128)(2,1)S(1)} %fusion.9.own_ref), custom_call_target="tpu_custom_call" | custom-call | tf_op jit(solution)/shard_map/attend/pallas_call | solution.py:203
  11.9 0.8 copy.27
  12.7 3.3 %all-to-all-start = ((bf16[4,128,128]{1,2,0:T(8,128)(2,1)}), bf16[4,128,128]{1,2,0:T(8,128)(2,1)S(1)}, u32[]{:S(2)}, u32[]{:S(2)}) async-start(bf16[4,128,128]{1,2,0:T(8,128)(2,1)} %copy.27), calls=%async_computation | async-start | bytes 262144 | tf_op jit(solution)/shard_map/all_to_all | solution.py:555
  16.1 0.0 copy-done.2
  16.1 0.1 copy.28
  16.2 0.0 copy-start.1
  16.2 0.1 eq.86
  16.3 0.1 eq.82
  16.5 0.6 reduce-window.6
  17.1 0.2 slice_reduce_fusion
  17.3 0.1 fusion.13
  17.4 0.1 reduce_sum.42
  17.6 0.1 copy.30
  17.6 0.1 fusion.10
  17.7 2.9 %all-to-all-done = bf16[4,128,128]{1,2,0:T(8,128)(2,1)S(1)} async-done(((bf16[4,128,128]{1,2,0:T(8,128)(2,1)}), bf16[4,128,128]{1,2,0:T(8,128)(2,1)S(1)}, u32[]{:S(2)}, u32[]{:S(2)}) %all-to-all-start) | async-done | bytes 131104 | tf_op jit(solution)/shard_map/all_to_all | solution.py:555
  20.6 0.0 copy-done
  20.6 1.6 multiply_reduce_fusion
  22.2 0.0 copy-done.1
  22.2 1.7 convolution_convert_fusion
  23.9 113.3 %dispatch.1.partial = bf16[32,40,2048]{2,1,0:T(8,128)(2,1)} custom-call(bf16[8,40,2048]{2,1,0:T(8,128)(2,1)} %bitcast.28, bf16[2048,1024]{1,0:T(8,128)(2,1)} %bitcast.29, bf16[2048,1024]{1,0:T(8,128)(2,1)} %bitcast.30, bf16[1024,2048]{1,0:T(8,128)(2,1)} %bitcast.31), custom_call_target="tpu_custom_call" | custom-call | tf_op jit(solution)/shard_map/dispatch/pallas_call | solution.py:485
  137.2 0.0 copy-start.3
  137.2 50.7 %combine.1 = bf16[8,40,2048]{2,1,0:T(8,128)(2,1)} custom-call(bf16[32,40,2048]{2,1,0:T(8,128)(2,1)} %dispatch.1.partial), custom_call_target="tpu_custom_call" | custom-call | tf_op jit(solution)/shard_map/combine/pallas_call | solution.py:516
  187.9 0.0 copy-done.3
  187.9 2.2 %fusion.2 = f32[128,2048]{1,0:T(8,128)S(1)} fusion(bf16[320,2048,1]{1,0,2:T(8,128)(2,1)} %bitcast.32, f32[128,2]{0,1:T(2,128)S(1)} %copy-done.3, s32[128,2]{0,1:T(2,128)S(1)} %multiply_add_fusion), kind=kOutput, calls=%fused_computation.5 | convolution fusion | flops 336412672 | bytes 2361344 | tf_op jit(solution)/shard_map/dot_general | solution.py:582
  190.1 0.9 add_convert_fusion
  (8 shorter events, 0.1 us)
Async XLA Ops:
  0.0 20.6 %copy-start = (bf16[512,2048]{1,0:T(8,128)(2,1)S(1)}, bf16[512,2048]{1,0:T(8,128)(2,1)}, u32[]{:S(2)}) copy-start(bf16[512,2048]{1,0:T(8,128)(2,1)} %param.17) | copy-start | bytes 6291460
  0.0 16.1 %copy-start.2 = (s32[128,2]{0,1:T(2,128)S(1)}, s32[128,2]{0,1:T(2,128)}, u32[]{:S(2)}) copy-start(s32[128,2]{0,1:T(2,128)} %param.19) | copy-start | bytes 3076
  12.7 7.9 %all-to-all-start = ((bf16[4,128,128]{1,2,0:T(8,128)(2,1)}), bf16[4,128,128]{1,2,0:T(8,128)(2,1)S(1)}, u32[]{:S(2)}, u32[]{:S(2)}) async-start(bf16[4,128,128]{1,2,0:T(8,128)(2,1)} %copy.27), calls=%async_computation | async-start | bytes 262144 | tf_op jit(solution)/shard_map/all_to_all | solution.py:555
  16.2 6.1 %copy-start.1 = (f32[2048]{0:T(1024)S(1)}, f32[2048]{0:T(1024)}, u32[]{:S(2)}) copy-start(f32[2048]{0:T(1024)} %param.18) | copy-start | bytes 24580
  137.2 50.8 %copy-start.3 = (f32[128,2]{0,1:T(2,128)S(1)}, f32[128,2]{0,1:T(2,128)}, u32[]{:S(2)}) copy-start(f32[128,2]{0,1:T(2,128)} %param.20) | copy-start | bytes 3076

commit v4 on v3

--- a/solution.py
+++ b/solution.py
@@ -222,11 +222,13 @@
 
 
 def dispatch_kernel(
-    n, groups, outgoing, gate_hbm, up_hbm, down_hbm, partial, rows, block, hidden, gate, up, down,
-    weight_sem, sp_sem, chip_sem, core_sem, recv_sem,
+    n, groups, outgoing, gate_hbm, up_hbm, down_hbm, back, partial, rows, block, hidden, gate, up,
+    down, pair, other, done, weight_sem, sp_sem, chip_sem, core_sem, recv_sem, pair_send, pair_recv,
+    chip_send, chip_recv, back_send, back_recv,
 ):
     me, my_t = lax.axis_index("sp"), lax.axis_index("tp")
-    mate = my_t + 1 - 2 * lax.rem(my_t, 2)
+    core = lax.rem(my_t, 2)
+    mate = my_t + 1 - 2 * core
     chips = groups // 2
     alike = [lax.rem(my_t + 2 * k, groups) for k in range(1, chips)]
     loads = [
@@ -308,67 +310,8 @@
 
         lax.fori_loop(0, down.shape[1] // BLOCK, features, 0)
 
-    def step(r, carry):
-        s = lax.rem(me + n - r, n)
-        arrived(my_t, s)
-        spread(s, rows.at[my_t * n + s])
-        relay(r - 1)
-        pl.when(r >= 2)(lambda: expert(r - 2))
-        return carry
-
-    lax.fori_loop(1, 2, step, 0)
-    for load in loads:
-        load.wait()
-    lax.fori_loop(2, n, step, 0)
-    relay(n - 1)
-
-    def last(r, carry):
-        expert(r)
-        return carry
-
-    lax.fori_loop(n - 2, n, last, 0)
-
-    def finish(s, carry):
-        pl.when(s >= 1)(lambda: to_expert(s).wait_send())
-        for k in range(chips - 1):
-            to_chip(k, s, outgoing.at[me]).wait_send()
-            to_mate(alike[k], s, outgoing.at[me]).wait_send()
-        to_mate(my_t, s, outgoing.at[me]).wait_send()
-        return carry
-
-    lax.fori_loop(0, n, finish, 0)
-
-
-def greet_all(n, me, mate, alike):
-    barrier = pltpu.get_barrier_semaphore()
-
-    def greet(device):
-        pl.semaphore_signal(barrier, inc=1, device_id=device, device_id_type=MESH)
-
-    def greet_sp(r, carry):
-        greet({"sp": lax.rem(me + r, n)})
-        return carry
-
-    lax.fori_loop(1, n, greet_sp, 0)
-    greet({"tp": mate})
-    for t in alike:
-        greet({"tp": t})
-    pl.semaphore_wait(barrier, n + len(alike))
-
-
-def combine_kernel(
-    n, groups, partial, back, pair, other, done, pair_send, pair_recv, chip_send, chip_recv,
-    back_send, back_recv,
-):
-    me, my_t = lax.axis_index("sp"), lax.axis_index("tp")
-    core = lax.rem(my_t, 2)
-    mate = my_t + 1 - 2 * core
-    chips = groups // 2
-    alike = [lax.rem(my_t + 2 * k, groups) for k in range(1, chips)]
-    greet_all(n, me, mate, alike)
-
     def home(r):
-        return lax.rem(me + 1 + r, n)
+        return lax.rem(me + n - r, n)
 
     def pair_copy(chip, r):
         return pltpu.make_async_remote_copy(
@@ -399,13 +342,6 @@
             device_id={"sp": home(r)},
             device_id_type=MESH,
         )
-
-    def start_pairs(r, carry):
-        for chip in range(chips):
-            pair_copy(chip, r).start()
-        return carry
-
-    lax.fori_loop(0, n, start_pairs, 0)
 
     def add_pairs(r):
         for chip in range(chips):
@@ -430,34 +366,66 @@
         for k in range(chips - 1):
             chip_copy(k, r).start()
 
-    lag = 1
-    for r in range(lag):
+    def multiply(r):
+        expert(r)
+        for chip in range(chips):
+            pair_copy(chip, r).start()
+
+    def sum_pairs(r):
         add_pairs(r)
         send_chips(r)
 
+    def give_own():
+        back[me] = add_chips(0)
+
+    def give_back(r):
+        done[r] = add_chips(r)
+        back_copy(r).start()
+
+    def flow(r):
+        pl.when(r < n)(lambda: multiply(r))
+        pl.when((r >= 1) & (r <= n))(lambda: sum_pairs(r - 1))
+        pl.when(r == 2)(give_own)
+        pl.when(r >= 3)(lambda: give_back(r - 2))
+
     def step(r, carry):
-        add_pairs(r)
-        send_chips(r)
-        done[r - lag] = add_chips(r - lag)
-        back_copy(r - lag).start()
-        return carry
-
-    lax.fori_loop(lag, n, step, 0)
-    for r in range(n - lag, n):
-        if r == n - 1:
-            back[me] = add_chips(r)
-        else:
-            done[r] = add_chips(r)
-            back_copy(r).start()
-
-    def finish(r, carry):
+        s = lax.rem(me + n - r, n)
+        arrived(my_t, s)
+        spread(s, rows.at[my_t * n + s])
+        relay(r - 1)
+        pl.when(r >= 2)(lambda: flow(r - 2))
+        return carry
+
+    lax.fori_loop(1, 2, step, 0)
+    for load in loads:
+        load.wait()
+    lax.fori_loop(2, n, step, 0)
+    relay(n - 1)
+
+    def last(r, carry):
+        flow(r)
+        return carry
+
+    lax.fori_loop(n - 2, n + 2, last, 0)
+
+    def finish(s, carry):
+        pl.when(s >= 1)(lambda: to_expert(s).wait_send())
+        for k in range(chips - 1):
+            to_chip(k, s, outgoing.at[me]).wait_send()
+            to_mate(alike[k], s, outgoing.at[me]).wait_send()
+        to_mate(my_t, s, outgoing.at[me]).wait_send()
+        return carry
+
+    lax.fori_loop(0, n, finish, 0)
+
+    def finish_sums(r, carry):
         for chip in range(chips):
             pair_copy(chip, r).wait_send()
         for k in range(chips - 1):
             chip_copy(k, r).wait_send()
         return carry
 
-    lax.fori_loop(0, n, finish, 0)
+    lax.fori_loop(0, n, finish_sums, 0)
 
     def finish_back(r, carry):
         back_copy(r).wait_send()
@@ -472,7 +440,24 @@
         ).wait_recv()
         return carry
 
-    lax.fori_loop(0, n - 1, finish_back, 0)
+    lax.fori_loop(1, n, finish_back, 0)
+
+
+def greet_all(n, me, mate, alike):
+    barrier = pltpu.get_barrier_semaphore()
+
+    def greet(device):
+        pl.semaphore_signal(barrier, inc=1, device_id=device, device_id_type=MESH)
+
+    def greet_sp(r, carry):
+        greet({"sp": lax.rem(me + r, n)})
+        return carry
+
+    lax.fori_loop(1, n, greet_sp, 0)
+    greet({"tp": mate})
+    for t in alike:
+        greet({"tp": t})
+    pl.semaphore_wait(barrier, n + len(alike))
 
 
 def dispatch(outgoing, gate, up, down):
@@ -480,48 +465,30 @@
     chips = groups // 2
     _, capacity, width = outgoing.shape
     units = gate.shape[1]
+    apart = max(1, chips - 1) * n
     vmem = pl.BlockSpec(memory_space=pltpu.VMEM)
     anywhere = pl.BlockSpec(memory_space=pl.ANY)
     return pl.pallas_call(
         functools.partial(dispatch_kernel, n, groups),
-        out_shape=jax.ShapeDtypeStruct((groups * n, capacity, width), outgoing.dtype),
+        out_shape=jax.ShapeDtypeStruct((n, capacity, width), outgoing.dtype),
         in_specs=[vmem, anywhere, anywhere, anywhere],
         out_specs=vmem,
         scratch_shapes=[
+            pltpu.VMEM((groups * n, capacity, width), outgoing.dtype),
             pltpu.VMEM((groups * n, capacity, width), outgoing.dtype),
             pltpu.VMEM((groups * capacity, width), outgoing.dtype),
             pltpu.VMEM((groups * capacity, units), outgoing.dtype),
             pltpu.VMEM((width, units), gate.dtype),
             pltpu.VMEM((width, units), up.dtype),
             pltpu.VMEM((units, width), down.dtype),
+            pltpu.VMEM((chips * n, capacity, width), outgoing.dtype),
+            pltpu.VMEM((apart, capacity, width), outgoing.dtype),
+            pltpu.VMEM((n, capacity, width), outgoing.dtype),
             pltpu.SemaphoreType.DMA((3,)),
             pltpu.SemaphoreType.DMA((n,)),
             pltpu.SemaphoreType.DMA((max(1, chips - 1) * n,)),
             pltpu.SemaphoreType.DMA((groups * n,)),
             pltpu.SemaphoreType.DMA((groups * n,)),
-        ],
-        compiler_params=pltpu.CompilerParams(
-            collective_id=1, has_side_effects=True, vmem_limit_bytes=60 * 1024 * 1024
-        ),
-        name="dispatch",
-    )(outgoing, gate, up, down)
-
-
-def combine(partial):
-    n, groups = lax.axis_size("sp"), lax.axis_size("tp")
-    chips = groups // 2
-    _, capacity, width = partial.shape
-    vmem = pl.BlockSpec(memory_space=pltpu.VMEM)
-    apart = max(1, chips - 1) * n
-    return pl.pallas_call(
-        functools.partial(combine_kernel, n, groups),
-        out_shape=jax.ShapeDtypeStruct((n, capacity, width), partial.dtype),
-        in_specs=[vmem],
-        out_specs=vmem,
-        scratch_shapes=[
-            pltpu.VMEM((chips * n, capacity, width), partial.dtype),
-            pltpu.VMEM((apart, capacity, width), partial.dtype),
-            pltpu.VMEM((n, capacity, width), partial.dtype),
             pltpu.SemaphoreType.DMA((chips * n,)),
             pltpu.SemaphoreType.DMA((chips * n,)),
             pltpu.SemaphoreType.DMA((apart,)),
@@ -530,10 +497,10 @@
             pltpu.SemaphoreType.DMA((n,)),
         ],
         compiler_params=pltpu.CompilerParams(
-            collective_id=2, has_side_effects=True, vmem_limit_bytes=56 * 1024 * 1024
+            collective_id=1, has_side_effects=True, vmem_limit_bytes=60 * 1024 * 1024
         ),
-        name="combine",
-    )(partial)
+        name="dispatch",
+    )(outgoing, gate, up, down)
 
 
 def shards(
@@ -572,13 +539,12 @@
     outgoing = jnp.einsum("ts,td->sd", placing, normed, preferred_element_type=jnp.float32).astype(
         jnp.bfloat16
     )
-    partial_rows = dispatch(
+    returned = dispatch(
         outgoing.reshape(sp_count, capacity, width_model),
         gate_weight[0],
         up_weight[0],
         down_weight[0],
-    )
-    returned = combine(partial_rows).reshape(-1, width_model)
+    ).reshape(-1, width_model)
     picked = jnp.dot(select, returned, preferred_element_type=jnp.float32).reshape(
         token_count, TOP, width_model
     )

time: 194 us -> 173 us (0.89); the launches traced: 191 us -> 172 us
  Pallas kernels: 173 us -> 156 us
    pallas_call x1 -> x0, Pallas kernels: 50.7 us -> none  [combine(): pl.pallas_call(functools.partial(combine_kernel, n, groups), out_shape=ja...]
    pallas_call x1, Pallas kernels: 113 us -> 146 us  [dispatch(): pl.pallas_call(functools.partial(dispatch_kernel, n, groups), out_shape=j...]
where the time goes in v4:
time: 173 us; the launch traced here: 172 us
  Pallas kernels  156 us (90%)
  matrix products  4.34 us (3%)
  other arithmetic  3.65 us (2%)
  starting transfers between devices  3.33 us (2%)
  waiting for transfers between devices  2.92 us (2%)
  local copies, waits for them, and re-layouts  2.44 us (1%)
    pallas_call x1, Pallas kernels, dispatch(): pl.pallas_call(functools.partial(dispatch_kernel, n, groups), out_shape=j...  146 us
    pallas_call x1, Pallas kernels, attend(): pl.pallas_call(functools.partial(attend_kernel, n, length, heads), out_sh...  9.13 us
  transfers between devices with their start and end apart: 1, of which 1 were waited for; matrix products, arithmetic and copies ran while one was open for 1% of the time, Pallas kernels for 0%

profile of v4, /device:TPU:0, one launch (start us, length us, event | category | flops | bytes accessed | tf_op | source)
XLA Modules:
  0.0 172.3 jit_solution(9454189203526080083)
XLA Ops:
  0.0 0.0 copy-start
  0.0 0.0 copy-start.3
  0.0 0.0 copy-start.1
  0.0 0.8 reshape.117
  0.9 0.9 broadcast_multiply_fusion
  1.8 1.0 fusion.9.own_ref
  2.8 9.1 %attend.1 = bf16[512,128]{1,0:T(8,128)(2,1)S(1)} custom-call(bf16[2,512,128]{2,1,0:T(8,128)(2,1)S(1)} %broadcast_select_fusion.q_ref, bf16[528,256]{1,0:T(8,128)(2,1)S(1)} %fusion.9.own_ref), custom_call_target="tpu_custom_call" | custom-call | tf_op jit(solution)/shard_map/attend/pallas_call | solution.py:203
  12.0 0.8 copy.27
  12.7 3.3 %all-to-all-start = ((bf16[4,128,128]{1,2,0:T(8,128)(2,1)}), bf16[4,128,128]{1,2,0:T(8,128)(2,1)S(1)}, u32[]{:S(2)}, u32[]{:S(2)}) async-start(bf16[4,128,128]{1,2,0:T(8,128)(2,1)} %copy.27), calls=%async_computation | async-start | bytes 262144 | tf_op jit(solution)/shard_map/all_to_all | solution.py:522
  16.1 0.0 copy-done.3
  16.1 0.1 copy.28
  16.2 0.0 copy-start.2
  16.2 0.1 eq.86
  16.3 0.1 eq.82
  16.5 0.6 reduce-window.6
  17.1 0.2 slice_reduce_fusion
  17.3 0.1 fusion.13
  17.4 0.1 reduce_sum.42
  17.6 0.1 copy.30
  17.6 0.1 fusion.10
  17.7 2.9 %all-to-all-done = bf16[4,128,128]{1,2,0:T(8,128)(2,1)S(1)} async-done(((bf16[4,128,128]{1,2,0:T(8,128)(2,1)}), bf16[4,128,128]{1,2,0:T(8,128)(2,1)S(1)}, u32[]{:S(2)}, u32[]{:S(2)}) %all-to-all-start) | async-done | bytes 131104 | tf_op jit(solution)/shard_map/all_to_all | solution.py:522
  20.6 0.0 copy-done
  20.6 0.0 copy-done.1
  20.6 0.5 multiply_reduce_fusion
  21.2 0.0 copy-done.2
  21.2 1.6 convolution_convert_fusion
  22.8 0.0 copy-start.4
  22.8 146.4 %dispatch.1 = bf16[8,40,2048]{2,1,0:T(8,128)(2,1)} custom-call(bf16[8,40,2048]{2,1,0:T(8,128)(2,1)} %bitcast.28, bf16[2048,1024]{1,0:T(8,128)(2,1)} %bitcast.29, bf16[2048,1024]{1,0:T(8,128)(2,1)} %bitcast.30, bf16[1024,2048]{1,0:T(8,128)(2,1)} %bitcast.31), custom_call_target="tpu_custom_call" | custom-call | tf_op jit(solution)/shard_map/dispatch/pallas_call | solution.py:471
  169.2 0.0 copy-done.4
  169.3 2.2 %fusion.2 = f32[128,2048]{1,0:T(8,128)S(1)} fusion(bf16[320,2048,1]{1,0,2:T(8,128)(2,1)} %bitcast.32, f32[128,2]{0,1:T(2,128)S(1)} %copy-done.4, s32[128,2]{0,1:T(2,128)S(1)} %multiply_add_fusion), kind=kOutput, calls=%fused_computation.5 | convolution fusion | flops 336412672 | bytes 2361344 | tf_op jit(solution)/shard_map/dot_general | solution.py:548
  171.4 0.9 add_convert_fusion
  (8 shorter events, 0.1 us)
Async XLA Ops:
  0.0 20.6 %copy-start = (bf16[512,2048]{1,0:T(8,128)(2,1)S(1)}, bf16[512,2048]{1,0:T(8,128)(2,1)}, u32[]{:S(2)}) copy-start(bf16[512,2048]{1,0:T(8,128)(2,1)} %param.17) | copy-start | bytes 6291460
  0.0 16.1 %copy-start.3 = (s32[128,2]{0,1:T(2,128)S(1)}, s32[128,2]{0,1:T(2,128)}, u32[]{:S(2)}) copy-start(s32[128,2]{0,1:T(2,128)} %param.19) | copy-start | bytes 3076
  0.0 20.6 %copy-start.1 = (bf16[128,2048]{1,0:T(8,128)(2,1)S(1)}, bf16[128,2048]{1,0:T(8,128)(2,1)}, u32[]{:S(2)}) copy-start(bf16[128,2048]{1,0:T(8,128)(2,1)} %param.16) | copy-start | bytes 1572868
  12.7 7.9 %all-to-all-start = ((bf16[4,128,128]{1,2,0:T(8,128)(2,1)}), bf16[4,128,128]{1,2,0:T(8,128)(2,1)S(1)}, u32[]{:S(2)}, u32[]{:S(2)}) async-start(bf16[4,128,128]{1,2,0:T(8,128)(2,1)} %copy.27), calls=%async_computation | async-start | bytes 262144 | tf_op jit(solution)/shard_map/all_to_all | solution.py:522
  16.2 5.0 %copy-start.2 = (f32[2048]{0:T(1024)S(1)}, f32[2048]{0:T(1024)}, u32[]{:S(2)}) copy-start(f32[2048]{0:T(1024)} %param.18) | copy-start | bytes 24580
  22.8 146.4 %copy-start.4 = (f32[128,2]{0,1:T(2,128)S(1)}, f32[128,2]{0,1:T(2,128)}, u32[]{:S(2)}) copy-start(f32[128,2]{0,1:T(2,128)} %param.20) | copy-start | bytes 3076
